TPU v7x, 32 devices: a whole 2x2x4 slice. The times are simulated.
32 devices in a mesh: fs: 8 (over z, y), tp: 4 (over x, core).
Axes of the slice: x: 2, y: 2, z: 4, core: 2. Of those that a mesh axis runs over, the one named last changes fastest.
Arguments:
- tokens: bfloat16 [4096, 2048], P(('fs', 'tp')), may hold values from -6 to 6
- norm_one: float32 [2048], replicated, may hold values from 0.1 to 1.9
- gate_one: bfloat16 [2048, 4608], P('fs', 'tp'), may hold values from -0.125 to 0.125
- up_one: bfloat16 [2048, 4608], P('fs', 'tp'), may hold values from -0.125 to 0.125
- down_one: bfloat16 [4608, 2048], P('tp', 'fs'), may hold values from -0.1875 to 0.1875
- norm_two: float32 [2048], replicated, may hold values from 0.1 to 1.9
- gate_two: bfloat16 [2048, 4608], P('fs', 'tp'), may hold values from -0.125 to 0.125
- up_two: bfloat16 [2048, 4608], P('fs', 'tp'), may hold values from -0.125 to 0.125
- down_two: bfloat16 [4608, 2048], P('tp', 'fs'), may hold values from -0.1875 to 0.1875
Outputs:
- result: bfloat16 [4096, 2048], P(('fs', 'tp'))
All inputs are finite; a program needn't handle non-finite values.
Results may differ from a plain program's by a relative error of at most 0.015.
Values may be sent and summed in bfloat16 or wider, within the bound.
A program may use at most 64 MiB of HBM per device.

v0:
```python
import jax
import jax.numpy as jnp
from jax import lax
from jax.sharding import PartitionSpec as P

eps = 1e-06


def normalize(rows, gain):
    values = rows.astype(jnp.float32)
    scaled = values * lax.rsqrt(jnp.mean(values * values, axis=-1, keepdims=True) + eps)
    return (scaled * gain).astype(jnp.bfloat16)


def hidden_units(rows, gain, gate_w, up_w):
    normed = normalize(rows, gain)
    gate_full, up_full = (
        lax.all_gather(gate_w, "fs", axis=0, tiled=True),
        lax.all_gather(up_w, "fs", axis=0, tiled=True),
    )
    gate_sum = jnp.dot(normed, gate_full, preferred_element_type=jnp.float32)
    up_sum = jnp.dot(normed, up_full, preferred_element_type=jnp.float32)
    return (jax.nn.silu(gate_sum) * up_sum).astype(jnp.bfloat16)


def down_terms(hidden, down_w):
    return jnp.dot(
        hidden, lax.all_gather(down_w, "fs", axis=1, tiled=True), preferred_element_type=jnp.float32
    )


def on_device(tokens, norm_one, gate_one, up_one, down_one, norm_two, gate_two, up_two, down_two):
    gathered = lax.all_gather(tokens, "tp", axis=0, tiled=True)
    first_terms = down_terms(hidden_units(gathered, norm_one, gate_one, up_one), down_one)
    summed = lax.psum(first_terms.astype(jnp.bfloat16), "tp").astype(jnp.float32)
    mid_group = (gathered.astype(jnp.float32) + 0.5 * summed).astype(jnp.bfloat16)
    mid_rows = lax.dynamic_slice_in_dim(
        mid_group, lax.axis_index("tp") * tokens.shape[0], tokens.shape[0], 0
    )
    second_terms = down_terms(hidden_units(mid_group, norm_two, gate_two, up_two), down_two)
    summed_two = lax.psum_scatter(
        second_terms.astype(jnp.bfloat16), "tp", scatter_dimension=0, tiled=True
    ).astype(jnp.float32)
    return (mid_rows.astype(jnp.float32) + 0.5 * summed_two).astype(jnp.bfloat16)


def solution(mesh):
    return jax.shard_map(
        on_device,
        mesh=mesh,
        in_specs=(
            P(("fs", "tp"), None),
            P(),
            P("fs", "tp"),
            P("fs", "tp"),
            P("tp", "fs"),
            P(),
            P("fs", "tp"),
            P("fs", "tp"),
            P("tp", "fs"),
        ),
        out_specs=P(("fs", "tp"), None),
        check_vma=False,
    )
```

profile of v0, /device:TPU:0, one launch (start us, length us, event | category | flops | bytes accessed | tf_op | source)
XLA Modules:
  0.0 631.1 jit_solution(18163117887727268943)
XLA Ops:
  6.5 0.0 copy-start.2
  6.5 0.0 all-gather.8.cloned.1.call-start
  6.5 0.7 all-gather.8.cloned.1.call-update
  7.3 0.0 all-gather.10.cloned.1.call-start
  7.3 0.7 all-gather.10.cloned.1.call-update
  8.0 0.0 all-gather.12.cloned.1.call-start
  8.1 0.7 all-gather.12.cloned.1.call-update
  8.7 0.0 all-gather.14.cloned.1.call-start
  8.8 0.5 all-gather.14.cloned.1.call-update
  9.3 0.0 all-reduce.2.cloned.1.call-start
  9.4 24.8 %all-gather.8.cloned.1.call-done = bf16[512,2048]{1,0:T(8,128)(2,1)} async-done(((bf16[128,2048]{1,0:T(8,128)(2,1)}), bf16[512,2048]{1,0:T(8,128)(2,1)}) %all-gather.8.cloned.1.call-update) | async-done | bytes 2097168 | tf_op jit(solution)/shard_map/all_gather | solution.py:33
  34.2 2.1 fusion.3
  36.3 0.0 copy-start
  36.3 79.5 %all-gather.10.cloned.1.call-done = bf16[2048,1152]{1,0:T(8,128)(2,1)} async-done(((bf16[256,1152]{1,0:T(8,128)(2,1)}), bf16[2048,1152]{1,0:T(8,128)(2,1)}) %all-gather.10.cloned.1.call-update) | async-done | bytes 4718608 | tf_op jit(solution)/shard_map/all_gather | solution.py:18
  115.8 0.0 copy-done.2
  115.8 7.3 %fusion.11 = f32[512,1152]{1,0:T(8,128)} fusion(bf16[2048,1152]{1,0:T(8,128)(2,1)} %all-gather.10.cloned.1.call-done, bf16[512,2048]{1,0:T(8,128)(2,1)} %all-gather.8.cloned.1.call-done, f32[2048]{0:T(1024)S(1)} %copy-done.2, f32[512]{0:T(512)S(1)} %add_rsqrt_fusion.1), kind=kOutput, calls=%fused_computation.19 | convolution fusion | flops 2420113408 | bytes 9185280 | tf_op jit(solution)/shard_map/dot_general | solution.py:21
  123.1 72.6 %all-gather.12.cloned.1.call-done = bf16[2048,1152]{1,0:T(8,128)(2,1)} async-done(((bf16[256,1152]{1,0:T(8,128)(2,1)}), bf16[2048,1152]{1,0:T(8,128)(2,1)}) %all-gather.12.cloned.1.call-update) | async-done | bytes 4718608 | tf_op jit(solution)/shard_map/all_gather | solution.py:19
  195.7 80.9 %all-gather.14.cloned.1.call-done = bf16[1152,2048]{1,0:T(8,128)(2,1)} async-done(((bf16[1152,256]{1,0:T(8,128)(2,1)}), bf16[1152,2048]{1,0:T(8,128)(2,1)}) %all-gather.14.cloned.1.call-update) | async-done | bytes 4718608 | tf_op jit(solution)/shard_map/all_gather | solution.py:28
  276.6 0.0 copy-done
  276.6 12.2 %convolution_convert_fusion.1 = bf16[512,2048]{1,0:T(8,128)(2,1)} fusion(bf16[1152,2048]{1,0:T(8,128)(2,1)} %all-gather.14.cloned.1.call-done, bf16[2048,1152]{1,0:T(8,128)(2,1)} %all-gather.12.cloned.1.call-done, f32[512,1152]{1,0:T(8,128)} %fusion.11, bf16[512,2048]{1,0:T(8,128)(2,1)S(1)} %copy-done, f32[2048]{0:T(1024)S(1)} %copy-done.2, ...), kind=kOutput, calls=%fused_computation.17 | convolution fusion | flops 4840620032 | bytes 16001024 | tf_op jit(solution)/shard_map/dot_general | solution.py:27
  288.7 0.0 all-reduce.2.cloned.1.call-update
  288.8 0.0 all-gather.16.cloned.1.call-start
  288.8 0.5 all-gather.16.cloned.1.call-update
  289.3 0.0 all-gather.18.cloned.1.call-start
  289.4 0.7 all-gather.18.cloned.1.call-update
  290.1 0.0 all-gather.20.cloned.1.call-start
  290.1 0.7 all-gather.20.cloned.1.call-update
  290.8 0.0 copy-start.3
  290.8 0.2 reduce-scatter.2.cloned.1.call-start
  291.1 47.4 %all-reduce.2.cloned.1.call-done = bf16[512,2048]{1,0:T(8,128)(2,1)} async-done(((bf16[512,2048]{1,0:T(8,128)(2,1)}), bf16[512,2048]{1,0:T(8,128)(2,1)}) %all-reduce.2.cloned.1.call-update) | async-done | bytes 2097168 | tf_op jit(solution)/shard_map/psum | solution.py:35
  338.5 4.0 fusion
  342.5 77.4 %all-gather.16.cloned.1.call-done = bf16[2048,1152]{1,0:T(8,128)(2,1)} async-done(((bf16[256,1152]{1,0:T(8,128)(2,1)}), bf16[2048,1152]{1,0:T(8,128)(2,1)}) %all-gather.16.cloned.1.call-update) | async-done | bytes 4718608 | tf_op jit(solution)/shard_map/all_gather | solution.py:18
  419.9 0.0 copy-done.3
  419.9 0.0 copy-start.1
  419.9 7.4 %fusion.15 = f32[512,1152]{1,0:T(8,128)} fusion(bf16[2048,1152]{1,0:T(8,128)(2,1)} %all-gather.16.cloned.1.call-done, bf16[512,2048]{1,0:T(8,128)(2,1)} %get-tuple-element.6, f32[2048]{0:T(1024)S(1)} %copy-done.3, f32[512]{0:T(512)S(1)} %add_rsqrt_fusion), kind=kOutput, calls=%fused_computation.20 | convolution fusion | flops 2420113408 | bytes 9185280 | tf_op jit(solution)/shard_map/dot_general | solution.py:21
  427.4 72.5 %all-gather.18.cloned.1.call-done = bf16[2048,1152]{1,0:T(8,128)(2,1)} async-done(((bf16[256,1152]{1,0:T(8,128)(2,1)}), bf16[2048,1152]{1,0:T(8,128)(2,1)}) %all-gather.18.cloned.1.call-update) | async-done | bytes 4718608 | tf_op jit(solution)/shard_map/all_gather | solution.py:19
  499.8 81.0 %all-gather.20.cloned.1.call-done = bf16[1152,2048]{1,0:T(8,128)(2,1)} async-done(((bf16[1152,256]{1,0:T(8,128)(2,1)}), bf16[1152,2048]{1,0:T(8,128)(2,1)}) %all-gather.20.cloned.1.call-update) | async-done | bytes 4718608 | tf_op jit(solution)/shard_map/all_gather | solution.py:28
  580.9 0.0 copy-done.1
  580.9 12.1 %convolution_convert_fusion = bf16[512,2048]{1,0:T(8,128)(2,1)} fusion(bf16[1152,2048]{1,0:T(8,128)(2,1)} %all-gather.20.cloned.1.call-done, bf16[2048,1152]{1,0:T(8,128)(2,1)} %all-gather.18.cloned.1.call-done, f32[512,1152]{1,0:T(8,128)} %fusion.15, bf16[512,2048]{1,0:T(8,128)(2,1)S(1)} %copy-done.1, f32[2048]{0:T(1024)S(1)} %copy-done.3, ...), kind=kOutput, calls=%fused_computation.16 | convolution fusion | flops 4840620032 | bytes 16001024 | tf_op jit(solution)/shard_map/dot_general | solution.py:27
  593.0 0.0 reduce-scatter.2.cloned.1.call-update
  593.1 29.5 %reduce-scatter.2.cloned.1.call-done = bf16[128,2048]{1,0:T(8,128)(2,1)} async-done(((bf16[512,2048]{1,0:T(8,128)(2,1)}), bf16[128,2048]{1,0:T(8,128)(2,1)}) %reduce-scatter.2.cloned.1.call-update) | async-done | bytes 524304 | tf_op jit(solution)/shard_map/reduce_scatter | solution.py:41
  622.5 2.0 add_convert_fusion
  (2 shorter events, 0.0 us)
Async XLA Ops:
  6.5 109.2 %copy-start.2 = (f32[2048]{0:T(1024)S(1)}, f32[2048]{0:T(1024)}, u32[]{:S(2)}) copy-start(f32[2048]{0:T(1024)} %param.10) | copy-start | bytes 24580
  6.5 27.7 %all-gather.8.cloned.1.call-start = ((), (), s32[]{:S(2)}) async-start(), calls=%async_computation.1 | async-start | bytes 2621440 | tf_op jit(solution)/shard_map/all_gather | solution.py:33
  7.3 108.5 %all-gather.10.cloned.1.call-start = ((), (), s32[]{:S(2)}) async-start(), calls=%async_computation.2 | async-start | bytes 5308416 | tf_op jit(solution)/shard_map/all_gather | solution.py:18
  8.0 187.7 %all-gather.12.cloned.1.call-start = ((), (), s32[]{:S(2)}) async-start(), calls=%async_computation.3 | async-start | bytes 5308416 | tf_op jit(solution)/shard_map/all_gather | solution.py:19
  8.7 267.8 %all-gather.14.cloned.1.call-start = ((), (), s32[]{:S(2)}) async-start(), calls=%async_computation.4 | async-start | bytes 5308416 | tf_op jit(solution)/shard_map/all_gather | solution.py:28
  9.3 329.1 %all-reduce.2.cloned.1.call-start = ((), (), s32[]{:S(2)}) async-start(), calls=%async_computation.5 | async-start | bytes 4194304 | tf_op jit(solution)/shard_map/psum | solution.py:35
  36.3 240.3 %copy-start = (bf16[512,2048]{1,0:T(8,128)(2,1)S(1)}, bf16[512,2048]{1,0:T(8,128)(2,1)}, u32[]{:S(2)}) copy-start(bf16[512,2048]{1,0:T(8,128)(2,1)} %all-gather.8.cloned.1.call-done) | copy-start | bytes 6291460
  288.8 131.2 %all-gather.16.cloned.1.call-start = ((), (), s32[]{:S(2)}) async-start(), calls=%async_computation.6 | async-start | bytes 5308416 | tf_op jit(solution)/shard_map/all_gather | solution.py:18
  289.3 210.5 %all-gather.18.cloned.1.call-start = ((), (), s32[]{:S(2)}) async-start(), calls=%async_computation.7 | async-start | bytes 5308416 | tf_op jit(solution)/shard_map/all_gather | solution.py:19
  290.1 290.8 %all-gather.20.cloned.1.call-start = ((), (), s32[]{:S(2)}) async-start(), calls=%async_computation.8 | async-start | bytes 5308416 | tf_op jit(solution)/shard_map/all_gather | solution.py:28
  290.8 129.1 %copy-start.3 = (f32[2048]{0:T(1024)S(1)}, f32[2048]{0:T(1024)}, u32[]{:S(2)}) copy-start(f32[2048]{0:T(1024)} %param.14) | copy-start | bytes 24580
  290.8 331.7 %reduce-scatter.2.cloned.1.call-start = ((), (), s32[]{:S(2)}) async-start(), calls=%async_computation.9 | async-start | bytes 2621440 | tf_op jit(solution)/shard_map/reduce_scatter | solution.py:41
  419.9 160.9 %copy-start.1 = (bf16[512,2048]{1,0:T(8,128)(2,1)S(1)}, bf16[512,2048]{1,0:T(8,128)(2,1)}, u32[]{:S(2)}) copy-start(bf16[512,2048]{1,0:T(8,128)(2,1)} %get-tuple-element.6) | copy-start | bytes 6291460
Sparse Core Ops, SparseCore 0:
  8.9 25.2 all-gather.7
  36.4 79.3 all-gather.9
  117.9 77.6 all-gather.11
  197.6 78.9 all-gather.13
  288.9 49.5 all-reduce.1
  340.5 79.3 all-gather.15
  422.1 77.6 all-gather.17
  501.9 78.9 all-gather.19
  593.2 29.3 reduce-scatter.1
where the time goes:
time: 631 us
  waiting for transfers between devices  570 us (90%)
  matrix products  39.1 us (6%)
  between operations  13.2 us (2%)
  other arithmetic  8.11 us (1%)
    all_gather x2, waiting for transfers between devices, down_terms(): lax.all_gather(down_w, 'fs', axis=1, tiled=True)  162 us
    all_gather x2, waiting for transfers between devices, hidden_units(): lax.all_gather(gate_w, 'fs', axis=0, tiled=True)  157 us
    all_gather x2, waiting for transfers between devices, hidden_units(): lax.all_gather(up_w, 'fs', axis=0, tiled=True)  145 us
    psum x1, waiting for transfers between devices, on_device(): lax.psum(first_terms.astype(jnp.bfloat16), 'tp').astype(jnp.float32)  47.4 us
    reduce_scatter x1, waiting for transfers between devices, on_device(): lax.psum_scatter(second_terms.astype(jnp.bfloat16), 'tp', scatter_dimensi...  29.5 us
    all_gather x1, waiting for transfers between devices, on_device(): gathered = lax.all_gather(tokens, 'tp', axis=0, tiled=True)  24.8 us
    dot_general x2, matrix products, down_terms(): jnp.dot(hidden, lax.all_gather(down_w, 'fs', axis=1, tiled=True), preferr...  24.3 us
    dot_general x2, matrix products, hidden_units(): gate_sum = jnp.dot(normed, gate_full, preferred_element_type=jnp.float32)  14.7 us
  transfers between devices with their start and end apart: 9, of which 9 were waited for; matrix products, arithmetic and copies ran while one was open for 3% of the time, Pallas kernels for 0%

commit v1 on v0

--- a/solution.py
+++ b/solution.py
@@ -15,7 +15,9 @@
 def hidden_units(rows, gain, gate_w, up_w):
     normed = normalize(rows, gain)
     gate_full, up_full = (
-        lax.all_gather(gate_w, "fs", axis=0, tiled=True),
+        jnp.concatenate(
+            lax.all_to_all(jnp.stack([gate_w] * lax.axis_size("fs")), "fs", 0, 0), axis=0
+        ),
         lax.all_gather(up_w, "fs", axis=0, tiled=True),
     )
     gate_sum = jnp.dot(normed, gate_full, preferred_element_type=jnp.float32)

time: 631 us -> 575 us (0.911)
  waiting for transfers between devices: 570 us -> 495 us
  starting transfers between devices: 0.49 us -> 12.5 us
  local copies, waits for them, and re-layouts: 0.02 us -> 6.56 us
    all_to_all x0 -> x2, waiting for transfers between devices: none -> 242 us  [hidden_units(): lax.all_to_all(jnp.stack([gate_w] * lax.axis_size('fs')), 'fs', 0, 0)]
    all_gather x2 -> x0, waiting for transfers between devices: 157 us -> none  [hidden_units(): lax.all_gather(gate_w, 'fs', axis=0, tiled=True)]
    all_gather x2, waiting for transfers between devices: 162 us -> 81.5 us  [down_terms(): lax.all_gather(down_w, 'fs', axis=1, tiled=True)]
    all_gather x2, waiting for transfers between devices: 145 us -> 82.7 us  [hidden_units(): lax.all_gather(up_w, 'fs', axis=0, tiled=True)]
    all_to_all x0 -> x2, starting transfers between devices: none -> 12 us  [hidden_units(): lax.all_to_all(jnp.stack([gate_w] * lax.axis_size('fs')), 'fs', 0, 0)]
    all_gather x1, waiting for transfers between devices: 24.8 us -> 14.2 us  [on_device(): gathered = lax.all_gather(tokens, 'tp', axis=0, tiled=True)]
    another operation x0 -> x2, local copies, waits for them, and re-layouts: none -> 6.53 us  [hidden_units(): jnp.stack([gate_w] * lax.axis_size('fs'))]
  transfers between devices with their start and end apart: 9 -> 9, of which waited for: 9 -> 8; matrix products, arithmetic and copies ran while one was open for 3% -> 5% of each run, Pallas kernels for 0% -> 0%
where the time goes in v1:
time: 575 us; the launch traced here: 574 us
  waiting for transfers between devices  495 us (86%)
  matrix products  39.2 us (7%)
  between operations  13.5 us (2%)
  starting transfers between devices  12.5 us (2%)
  other arithmetic  8.1 us (1%)
  local copies, waits for them, and re-layouts  6.56 us (1%)
    all_to_all x2, waiting for transfers between devices, hidden_units(): lax.all_to_all(jnp.stack([gate_w] * lax.axis_size('fs')), 'fs', 0, 0)  242 us
    all_gather x2, waiting for transfers between devices, hidden_units(): lax.all_gather(up_w, 'fs', axis=0, tiled=True)  82.7 us
    all_gather x2, waiting for transfers between devices, down_terms(): lax.all_gather(down_w, 'fs', axis=1, tiled=True)  81.5 us
    psum x1, waiting for transfers between devices, on_device(): lax.psum(first_terms.astype(jnp.bfloat16), 'tp').astype(jnp.float32)  41.1 us
    reduce_scatter x1, waiting for transfers between devices, on_device(): lax.psum_scatter(second_terms.astype(jnp.bfloat16), 'tp', scatter_dimensi...  29.5 us
    dot_general x2, matrix products, down_terms(): jnp.dot(hidden, lax.all_gather(down_w, 'fs', axis=1, tiled=True), preferr...  24.3 us
    dot_general x2, matrix products, hidden_units(): gate_sum = jnp.dot(normed, gate_full, preferred_element_type=jnp.float32)  14.9 us
    all_gather x1, waiting for transfers between devices, on_device(): gathered = lax.all_gather(tokens, 'tp', axis=0, tiled=True)  14.2 us
  transfers between devices with their start and end apart: 9, of which 8 were waited for; matrix products, arithmetic and copies ran while one was open for 5% of the time, Pallas kernels for 0%

profile of v1, /device:TPU:0, one launch (start us, length us, event | category | flops | bytes accessed | tf_op | source)
XLA Modules:
  0.0 574.4 jit_solution(13343769217725946476)
XLA Ops:
  6.5 0.0 all-gather.6.cloned.1.call-start
  6.5 0.7 all-gather.6.cloned.1.call-update
  7.3 0.0 all-gather.10.cloned.1.call-start
  7.3 0.7 all-gather.10.cloned.1.call-update
  8.0 3.8 stack.4
  11.8 0.0 copy-start.3
  11.8 7.4 %all-to-all-start = ((bf16[8,256,1152]{2,1,0:T(8,128)(2,1)}), bf16[8,256,1152]{2,1,0:T(8,128)(2,1)}, u32[]{:S(2)}, u32[]{:S(2)}) async-start(bf16[8,256,1152]{2,1,0:T(8,128)(2,1)} %stack.4), calls=%async_computation | async-start | bytes 9437184 | tf_op jit(solution)/shard_map/all_to_all | solution.py:19
  19.2 0.0 all-gather.8.cloned.1.call-start
  19.3 0.7 all-gather.8.cloned.1.call-update
  20.0 0.0 all-reduce.2.cloned.1.call-start
  20.0 14.2 %all-gather.6.cloned.1.call-done = bf16[512,2048]{1,0:T(8,128)(2,1)} async-done(((bf16[128,2048]{1,0:T(8,128)(2,1)}), bf16[512,2048]{1,0:T(8,128)(2,1)}) %all-gather.6.cloned.1.call-update) | async-done | bytes 2097168 | tf_op jit(solution)/shard_map/all_gather | solution.py:35
  34.2 2.1 fusion.3
  36.3 141.4 %all-to-all-done = bf16[8,256,1152]{2,1,0:T(8,128)(2,1)} async-done(((bf16[8,256,1152]{2,1,0:T(8,128)(2,1)}), bf16[8,256,1152]{2,1,0:T(8,128)(2,1)}, u32[]{:S(2)}, u32[]{:S(2)}) %all-to-all-start) | async-done | bytes 4718624 | tf_op jit(solution)/shard_map/all_to_all | solution.py:19
  177.7 0.0 copy-done.3
  177.7 0.0 copy-start
  177.7 7.4 %fusion.11 = f32[512,1152]{1,0:T(8,128)} fusion(bf16[2048,1152]{1,0:T(8,128)(2,1)} %bitcast, bf16[512,2048]{1,0:T(8,128)(2,1)} %all-gather.6.cloned.1.call-done, f32[2048]{0:T(1024)S(1)} %copy-done.3, f32[512]{0:T(512)S(1)} %add_rsqrt_fusion.1), kind=kOutput, calls=%fused_computation.19 | convolution fusion | flops 2420113408 | bytes 9185280 | tf_op jit(solution)/shard_map/dot_general | solution.py:23
  185.1 0.0 copy-start.2
  185.1 0.0 all-gather.10.cloned.1.call-done
  185.1 76.4 %all-gather.8.cloned.1.call-done = bf16[2048,1152]{1,0:T(8,128)(2,1)} async-done(((bf16[256,1152]{1,0:T(8,128)(2,1)}), bf16[2048,1152]{1,0:T(8,128)(2,1)}) %all-gather.8.cloned.1.call-update) | async-done | bytes 4718608 | tf_op jit(solution)/shard_map/all_gather | solution.py:21
  261.5 0.0 copy-done
  261.5 12.2 %convolution_convert_fusion.1 = bf16[512,2048]{1,0:T(8,128)(2,1)} fusion(bf16[1152,2048]{1,0:T(8,128)(2,1)} %all-gather.10.cloned.1.call-done, bf16[2048,1152]{1,0:T(8,128)(2,1)} %all-gather.8.cloned.1.call-done, f32[512,1152]{1,0:T(8,128)} %fusion.11, bf16[512,2048]{1,0:T(8,128)(2,1)S(1)} %copy-done, f32[2048]{0:T(1024)S(1)} %copy-done.3, ...), kind=kOutput, calls=%fused_computation.17 | convolution fusion | flops 4840620032 | bytes 16001024 | tf_op jit(solution)/shard_map/dot_general | solution.py:29
  273.7 0.0 all-reduce.2.cloned.1.call-update
  273.7 0.0 all-gather.12.cloned.1.call-start
  273.7 0.5 all-gather.12.cloned.1.call-update
  274.3 0.0 copy-done.2
  274.3 2.7 stack.5
  277.0 4.6 all-to-all-start.1
  281.6 0.0 copy-start.4
  281.6 0.0 all-gather.14.cloned.1.call-start
  281.7 0.5 all-gather.14.cloned.1.call-update
  282.2 0.2 reduce-scatter.2.cloned.1.call-start
  282.4 41.1 %all-reduce.2.cloned.1.call-done = bf16[512,2048]{1,0:T(8,128)(2,1)} async-done(((bf16[512,2048]{1,0:T(8,128)(2,1)}), bf16[512,2048]{1,0:T(8,128)(2,1)}) %all-reduce.2.cloned.1.call-update) | async-done | bytes 2097168 | tf_op jit(solution)/shard_map/psum | solution.py:37
  323.6 4.0 fusion
  327.6 101.0 %all-to-all-done.1 = bf16[8,256,1152]{2,1,0:T(8,128)(2,1)} async-done(((bf16[8,256,1152]{2,1,0:T(8,128)(2,1)}), bf16[8,256,1152]{2,1,0:T(8,128)(2,1)}, u32[]{:S(2)}, u32[]{:S(2)}) %all-to-all-start.1) | async-done | bytes 4718624 | tf_op jit(solution)/shard_map/all_to_all | solution.py:19
  428.6 0.0 copy-done.4
  428.6 0.0 copy-start.1
  428.6 7.5 %fusion.15 = f32[512,1152]{1,0:T(8,128)} fusion(bf16[2048,1152]{1,0:T(8,128)(2,1)} %bitcast.1, bf16[512,2048]{1,0:T(8,128)(2,1)} %get-tuple-element.6, f32[2048]{0:T(1024)S(1)} %copy-done.4, f32[512]{0:T(512)S(1)} %add_rsqrt_fusion), kind=kOutput, calls=%fused_computation.20 | convolution fusion | flops 2420113408 | bytes 9185280 | tf_op jit(solution)/shard_map/dot_general | solution.py:23
  436.1 6.3 %all-gather.12.cloned.1.call-done = bf16[2048,1152]{1,0:T(8,128)(2,1)} async-done(((bf16[256,1152]{1,0:T(8,128)(2,1)}), bf16[2048,1152]{1,0:T(8,128)(2,1)}) %all-gather.12.cloned.1.call-update) | async-done | bytes 4718608 | tf_op jit(solution)/shard_map/all_gather | solution.py:21
  442.4 81.5 %all-gather.14.cloned.1.call-done = bf16[1152,2048]{1,0:T(8,128)(2,1)} async-done(((bf16[1152,256]{1,0:T(8,128)(2,1)}), bf16[1152,2048]{1,0:T(8,128)(2,1)}) %all-gather.14.cloned.1.call-update) | async-done | bytes 4718608 | tf_op jit(solution)/shard_map/all_gather | solution.py:30
  523.9 0.0 copy-done.1
  523.9 12.1 %convolution_convert_fusion = bf16[512,2048]{1,0:T(8,128)(2,1)} fusion(bf16[1152,2048]{1,0:T(8,128)(2,1)} %all-gather.14.cloned.1.call-done, bf16[2048,1152]{1,0:T(8,128)(2,1)} %all-gather.12.cloned.1.call-done, f32[512,1152]{1,0:T(8,128)} %fusion.15, bf16[512,2048]{1,0:T(8,128)(2,1)S(1)} %copy-done.1, f32[2048]{0:T(1024)S(1)} %copy-done.4, ...), kind=kOutput, calls=%fused_computation.16 | convolution fusion | flops 4840620032 | bytes 16001024 | tf_op jit(solution)/shard_map/dot_general | solution.py:29
  536.0 0.0 reduce-scatter.2.cloned.1.call-update
  536.1 29.5 %reduce-scatter.2.cloned.1.call-done = bf16[128,2048]{1,0:T(8,128)(2,1)} async-done(((bf16[512,2048]{1,0:T(8,128)(2,1)}), bf16[128,2048]{1,0:T(8,128)(2,1)}) %reduce-scatter.2.cloned.1.call-update) | async-done | bytes 524304 | tf_op jit(solution)/shard_map/reduce_scatter | solution.py:43
  565.5 2.0 add_convert_fusion
  (2 shorter events, 0.0 us)
Async XLA Ops:
  6.5 27.7 %all-gather.6.cloned.1.call-start = ((), (), s32[]{:S(2)}) async-start(), calls=%async_computation.3 | async-start | bytes 2621440 | tf_op jit(solution)/shard_map/all_gather | solution.py:35
  7.3 177.9 %all-gather.10.cloned.1.call-start = ((), (), s32[]{:S(2)}) async-start(), calls=%async_computation.5 | async-start | bytes 5308416 | tf_op jit(solution)/shard_map/all_gather | solution.py:30
  11.8 165.9 %copy-start.3 = (f32[2048]{0:T(1024)S(1)}, f32[2048]{0:T(1024)}, u32[]{:S(2)}) copy-start(f32[2048]{0:T(1024)} %param.10) | copy-start | bytes 24580
  11.8 165.9 %all-to-all-start = ((bf16[8,256,1152]{2,1,0:T(8,128)(2,1)}), bf16[8,256,1152]{2,1,0:T(8,128)(2,1)}, u32[]{:S(2)}, u32[]{:S(2)}) async-start(bf16[8,256,1152]{2,1,0:T(8,128)(2,1)} %stack.4), calls=%async_computation | async-start | bytes 9437184 | tf_op jit(solution)/shard_map/all_to_all | solution.py:19
  19.2 242.2 %all-gather.8.cloned.1.call-start = ((), (), s32[]{:S(2)}) async-start(), calls=%async_computation.4 | async-start | bytes 5308416 | tf_op jit(solution)/shard_map/all_gather | solution.py:21
  20.0 303.6 %all-reduce.2.cloned.1.call-start = ((), (), s32[]{:S(2)}) async-start(), calls=%async_computation.6 | async-start | bytes 4194304 | tf_op jit(solution)/shard_map/psum | solution.py:37
  177.7 83.8 %copy-start = (bf16[512,2048]{1,0:T(8,128)(2,1)S(1)}, bf16[512,2048]{1,0:T(8,128)(2,1)}, u32[]{:S(2)}) copy-start(bf16[512,2048]{1,0:T(8,128)(2,1)} %all-gather.6.cloned.1.call-done) | copy-start | bytes 6291460
  185.1 89.2 %copy-start.2 = (bf16[256,1152]{1,0:T(8,128)(2,1)S(1)}, bf16[256,1152]{1,0:T(8,128)(2,1)}, u32[]{:S(2)}) copy-start(bf16[256,1152]{1,0:T(8,128)(2,1)} %param.15) | copy-start | bytes 1769476
  273.7 168.7 %all-gather.12.cloned.1.call-start = ((), (), s32[]{:S(2)}) async-start(), calls=%async_computation.7 | async-start | bytes 5308416 | tf_op jit(solution)/shard_map/all_gather | solution.py:21
  277.0 151.6 %all-to-all-start.1 = ((bf16[8,256,1152]{2,1,0:T(8,128)(2,1)}), bf16[8,256,1152]{2,1,0:T(8,128)(2,1)}, u32[]{:S(2)}, u32[]{:S(2)}) async-start(bf16[8,256,1152]{2,1,0:T(8,128)(2,1)} %stack.5), calls=%async_computation.1 | async-start | bytes 9437184 | tf_op jit(solution)/shard_map/all_to_all | solution.py:19
  281.6 147.0 %copy-start.4 = (f32[2048]{0:T(1024)S(1)}, f32[2048]{0:T(1024)}, u32[]{:S(2)}) copy-start(f32[2048]{0:T(1024)} %param.14) | copy-start | bytes 24580
  281.6 242.3 %all-gather.14.cloned.1.call-start = ((), (), s32[]{:S(2)}) async-start(), calls=%async_computation.8 | async-start | bytes 5308416 | tf_op jit(solution)/shard_map/all_gather | solution.py:30
  282.2 283.3 %reduce-scatter.2.cloned.1.call-start = ((), (), s32[]{:S(2)}) async-start(), calls=%async_computation.9 | async-start | bytes 2621440 | tf_op jit(solution)/shard_map/reduce_scatter | solution.py:43
  428.6 95.3 %copy-start.1 = (bf16[512,2048]{1,0:T(8,128)(2,1)S(1)}, bf16[512,2048]{1,0:T(8,128)(2,1)}, u32[]{:S(2)}) copy-start(bf16[512,2048]{1,0:T(8,128)(2,1)} %get-tuple-element.6) | copy-start | bytes 6291460
Sparse Core Ops, SparseCore 0:
  8.9 25.2 all-gather.5
  36.2 144.6 all-gather.9
  183.2 78.2 all-gather.7
  273.8 49.7 all-reduce.1
  325.6 116.7 all-gather.11
  444.3 79.5 all-gather.13
  536.2 29.3 reduce-scatter.1
